TPU v7x, 32 devices: a whole 2x2x4 slice. The times are simulated.
32 devices in a mesh: fs: 8 (over z, y), tp: 4 (over x, core).
Axes of the slice: x: 2, y: 2, z: 4, core: 2. Of those that a mesh axis runs over, the one named last changes fastest.
Arguments:
- inputs: bfloat16 [9216, 2048], P('fs'), may hold values from -6 to 6
- gate_cot: bfloat16 [9216, 4096], P('fs', 'tp'), may hold values from -0.0546875 to 0.0546875
- state_cot: bfloat16 [9216, 1024], P('fs', 'tp'), may hold values from -0.0546875 to 0.0546875
- gate_weight: float32 [2048, 4096], P('fs', 'tp'), may hold values from -0.75 to 0.75
- state_weight: float32 [2048, 1024], P('fs', 'tp'), may hold values from -0.75 to 0.75
- gate_factor: bfloat16 [2048, 256], P('fs'), may hold values from -0.375 to 0.375
- state_factor: bfloat16 [2048, 256], P('fs'), may hold values from -0.375 to 0.375
- gate_first: float32 [256, 4096], P('fs', 'tp'), may hold values from -6 to 6
- gate_second: float32 [256, 4096], P('fs', 'tp'), may hold values from 0.3 to 3
- state_first: float32 [256, 1024], P('fs', 'tp'), may hold values from -6 to 6
- state_second: float32 [256, 1024], P('fs', 'tp'), may hold values from 0.3 to 3
Outputs:
- new_gate_weight: float32 [2048, 4096], P('fs', 'tp')
- new_state_weight: float32 [2048, 1024], P('fs', 'tp')
- gate_copy: bfloat16 [2048, 4096], P(None, 'tp')
- state_copy: bfloat16 [2048, 1024], P(None, 'tp')
- new_gate_first: float32 [256, 4096], P('fs', 'tp')
- new_gate_second: float32 [256, 4096], P('fs', 'tp')
- new_state_first: float32 [256, 1024], P('fs', 'tp')
- new_state_second: float32 [256, 1024], P('fs', 'tp')
All inputs are finite; a program needn't handle non-finite values.
Results may differ from a plain program's by a relative error of at most 0.004.
Values may be sent and summed in bfloat16 or wider, within the bound.
No kernel may reach another device: no remote copies, remote signals or barrier semaphores. Data moves between devices by JAX's collectives and lax.ppermute only.
A program may use at most 128 MiB of HBM per device.

v0:
```python
import jax
import jax.numpy as jnp
from jax import lax
from jax.sharding import PartitionSpec as P

D = 2048
DI = 4096
BW = 1024


def lifted_product(inputs, factor, cot):
    lifted = jnp.dot(inputs, factor, preferred_element_type=jnp.float32)
    upper = lifted.astype(jnp.bfloat16)
    lower = (lifted - upper.astype(jnp.float32)).astype(jnp.bfloat16)
    first_part = jnp.einsum("tr,tc->rc", upper, cot, preferred_element_type=jnp.float32)
    return first_part + jnp.einsum("tr,tc->rc", lower, cot, preferred_element_type=jnp.float32)


def per_device(
    inputs,
    gate_cot,
    state_cot,
    gate_weight,
    state_weight,
    gate_factor,
    state_factor,
    gate_first,
    gate_second,
    state_first,
    state_second,
):
    gate_cols = gate_cot.shape[1]
    whole_gate, whole_state = (
        lax.all_gather(gate_factor, "fs", axis=0, tiled=True),
        lax.all_gather(state_factor, "fs", axis=0, tiled=True),
    )
    gate_part = lifted_product(inputs, whole_gate, gate_cot)
    state_part = lifted_product(inputs, whole_state, state_cot)
    partial_proj = jnp.concatenate([gate_part, state_part], 1)
    projection = lax.psum_scatter(partial_proj, "fs", scatter_dimension=0, tiled=True)
    first_old = jnp.concatenate([gate_first, state_first], 1)
    second_old = jnp.concatenate([gate_second, state_second], 1)
    first_new = 0.8 * first_old + 0.2 * projection
    second_new = 0.9 * second_old + 0.1 * projection * projection
    direction = (first_new / jnp.sqrt(second_new)).astype(jnp.bfloat16)
    all_dirs = lax.all_gather(direction, "fs", axis=0, tiled=True)
    gate_full = jnp.dot(gate_factor, all_dirs[:, :gate_cols], preferred_element_type=jnp.float32)
    state_full = jnp.dot(state_factor, all_dirs[:, gate_cols:], preferred_element_type=jnp.float32)
    gate_sq, state_sq = lax.psum(
        (jnp.sum(gate_full * gate_full), jnp.sum(state_full * state_full)), ("fs", "tp")
    )
    gate_scale = 0.02 / jnp.sqrt(gate_sq / (D * DI) + 0.25)
    state_scale = 0.02 / jnp.sqrt(state_sq / (D * BW) + 0.25)
    gate_new = gate_weight - gate_scale * gate_full
    state_new = state_weight - state_scale * state_full
    gate_copy, state_copy = (
        lax.all_gather(gate_new.astype(jnp.bfloat16), "fs", axis=0, tiled=True),
        lax.all_gather(state_new.astype(jnp.bfloat16), "fs", axis=0, tiled=True),
    )
    return (
        gate_new,
        state_new,
        gate_copy,
        state_copy,
        first_new[:, :gate_cols],
        second_new[:, :gate_cols],
        first_new[:, gate_cols:],
        second_new[:, gate_cols:],
    )


def solution(mesh):
    return jax.shard_map(
        per_device,
        mesh=mesh,
        in_specs=(
            P("fs", None),
            P("fs", "tp"),
            P("fs", "tp"),
            P("fs", "tp"),
            P("fs", "tp"),
            P("fs", None),
            P("fs", None),
            P("fs", "tp"),
            P("fs", "tp"),
            P("fs", "tp"),
            P("fs", "tp"),
        ),
        out_specs=(
            P("fs", "tp"),
            P("fs", "tp"),
            P(None, "tp"),
            P(None, "tp"),
            P("fs", "tp"),
            P("fs", "tp"),
            P("fs", "tp"),
            P("fs", "tp"),
        ),
        check_vma=False,
    )
```

profile of v0, /device:TPU:0, one launch (start us, length us, event | category | flops | bytes accessed | tf_op | source)
XLA Modules:
  0.0 370.5 jit_solution(9867147324126327805)
XLA Ops:
  7.2 0.7 all-gather.5.cloned.1.call-update
  8.0 0.7 all-gather.7.cloned.1.call-update
  8.7 44.4 %all-gather.5.cloned.1.call-done = bf16[2048,256]{1,0:T(8,128)(2,1)} async-done(((bf16[256,256]{1,0:T(8,128)(2,1)}), bf16[2048,256]{1,0:T(8,128)(2,1)}) %all-gather.5.cloned.1.call-update) | async-done | bytes 1048592 | tf_op jit(solution)/shard_map/all_gather | solution.py:34
  53.2 4.1 %fusion.16 = f32[1152,256]{1,0:T(8,128)S(1)} fusion(bf16[1152,2048]{1,0:T(8,128)(2,1)} %param.11, bf16[2048,256]{1,0:T(8,128)(2,1)} %all-gather.5.cloned.1.call-done), kind=kOutput, calls=%fused_computation.27 | convolution fusion | flops 1207959552 | bytes 6946816 | tf_op jit(solution)/shard_map/dot_general | solution.py:12
  57.2 0.9 fusion.6
  58.1 0.9 convolution_add_fusion
  59.0 35.3 %all-gather.7.cloned.1.call-done = bf16[2048,256]{1,0:T(8,128)(2,1)} async-done(((bf16[256,256]{1,0:T(8,128)(2,1)}), bf16[2048,256]{1,0:T(8,128)(2,1)}) %all-gather.7.cloned.1.call-update) | async-done | bytes 1048592 | tf_op jit(solution)/shard_map/all_gather | solution.py:35
  94.3 4.1 %fusion.17 = f32[1152,256]{1,0:T(8,128)S(1)} fusion(bf16[1152,2048]{1,0:T(8,128)(2,1)} %param.11, bf16[2048,256]{1,0:T(8,128)(2,1)} %all-gather.7.cloned.1.call-done), kind=kOutput, calls=%fused_computation.28 | convolution fusion | flops 1207959552 | bytes 6946816 | tf_op jit(solution)/shard_map/dot_general | solution.py:12
  98.4 0.4 fusion.3
  98.8 0.4 convolution_add_fusion.1
  99.2 1.2 pad_maximum_fusion
  100.4 0.8 copy-done.5
  101.3 0.8 copy.22
  102.1 62.2 %reduce-scatter.2.cloned.1.call-done = f32[32,1280]{1,0:T(8,128)} async-done(((f32[256,1280]{1,0:T(8,128)}), f32[32,1280]{1,0:T(8,128)}) %reduce-scatter.2.cloned.1.call-update) | async-done | bytes 163856 | tf_op jit(solution)/shard_map/reduce_scatter | solution.py:40
  164.4 1.7 multiply_convert_fusion
  166.1 32.1 %all_gather.17 = bf16[256,1280]{1,0:T(8,128)(2,1)S(1)} all-gather(bf16[32,1280]{1,0:T(8,128)(2,1)S(1)} %get-tuple-element.22), channel_id=1, replica_groups=mesh['fs'=8,'tp'=4] {'fs'}, dimensions={0}, use_global_device_ids=true | all-gather | bytes 737280 | tf_op jit(solution)/shard_map/all_gather | solution.py:46
  198.2 1.1 multiply_reduce_fusion
  199.2 1.5 multiply_reduce_fusion.1
  200.8 37.5 %all-reduce = (f32[]{:T(128)}, f32[]{:T(128)}) all-reduce(f32[]{:T(128)} %get-tuple-element.25, f32[]{:T(128)} %get-tuple-element.27), channel_id=1, replica_groups=mesh['fs'=8,'tp'=4] {'fs','tp'}, use_global_device_ids=true, to_apply=%region_2.0 | all-reduce | flops 2 | bytes 16 | tf_op jit(solution)/shard_map/psum | solution.py:49
  238.9 1.8 fusion.12
  240.8 2.5 copy.21
  244.0 2.5 fusion.13
  246.6 1.7 slice.26
  248.2 1.4 slice.28
  249.6 1.6 slice.27
  251.2 1.4 slice.29
  252.6 1.8 copy.24
  254.4 1.3 copy.23
  255.7 25.7 %all-gather.11.cloned.1.call-done = bf16[2048,256]{0,1:T(8,128)(2,1)} async-done(((bf16[256,256]{0,1:T(8,128)(2,1)}), bf16[2048,256]{0,1:T(8,128)(2,1)}) %all-gather.11.cloned.1.call-update) | async-done | bytes 1048592 | tf_op jit(solution)/shard_map/all_gather | solution.py:58
  281.4 2.3 copy.26
  283.7 73.9 %all-gather.9.cloned.1.call-done = bf16[2048,1024]{0,1:T(8,128)(2,1)} async-done(((bf16[256,1024]{0,1:T(8,128)(2,1)}), bf16[2048,1024]{0,1:T(8,128)(2,1)}) %all-gather.9.cloned.1.call-update) | async-done | bytes 4194320 | tf_op jit(solution)/shard_map/all_gather | solution.py:57
  357.5 6.4 %copy.25 = bf16[2048,1024]{1,0:T(8,128)(2,1)} copy(bf16[2048,1024]{0,1:T(8,128)(2,1)} %all-gather.9.cloned.1.call-done) | data formatting | bytes 8388608
  (27 shorter events, 0.3 us)
Async XLA Ops:
  7.2 50.0 %copy-start = (bf16[1152,1024]{1,0:T(8,128)(2,1)S(1)}, bf16[1152,1024]{1,0:T(8,128)(2,1)}, u32[]{:S(2)}) copy-start(bf16[1152,1024]{1,0:T(8,128)(2,1)} %param.12) | copy-start | bytes 7077892
  7.2 46.0 %all-gather.5.cloned.1.call-start = ((), (), s32[]{:S(2)}) async-start(), calls=%async_computation.1 | async-start | bytes 1179648 | tf_op jit(solution)/shard_map/all_gather | solution.py:34
  7.9 86.4 %all-gather.7.cloned.1.call-start = ((), (), s32[]{:S(2)}) async-start(), calls=%async_computation.2 | async-start | bytes 1179648 | tf_op jit(solution)/shard_map/all_gather | solution.py:35
  8.7 155.7 %reduce-scatter.2.cloned.1.call-start = ((), (), s32[]{:S(2)}) async-start(), calls=%async_computation.3 | async-start | bytes 1474560 | tf_op jit(solution)/shard_map/reduce_scatter | solution.py:40
  94.3 4.1 %copy-start.2 = (bf16[1152,256]{1,0:T(8,128)(2,1)S(1)}, bf16[1152,256]{1,0:T(8,128)(2,1)}, u32[]{:S(2)}) copy-start(bf16[1152,256]{1,0:T(8,128)(2,1)} %param.13) | copy-start | bytes 1769476
  100.3 0.9 copy-start.5
  100.3 64.0 %copy-start.6 = (f32[32,1024]{1,0:T(8,128)S(1)}, f32[32,1024]{1,0:T(8,128)}, u32[]{:S(2)}) copy-start(f32[32,1024]{1,0:T(8,128)} %param.19) | copy-start | bytes 393220
  100.3 64.0 %copy-start.7 = (f32[32,1024]{1,0:T(8,128)S(1)}, f32[32,1024]{1,0:T(8,128)}, u32[]{:S(2)}) copy-start(f32[32,1024]{1,0:T(8,128)} %param.18) | copy-start | bytes 393220
  100.3 64.0 %copy-start.8 = (f32[32,256]{1,0:T(8,128)S(1)}, f32[32,256]{1,0:T(8,128)}, u32[]{:S(2)}) copy-start(f32[32,256]{1,0:T(8,128)} %param.21) | copy-start | bytes 98308
  100.3 64.0 %copy-start.9 = (f32[32,256]{1,0:T(8,128)S(1)}, f32[32,256]{1,0:T(8,128)}, u32[]{:S(2)}) copy-start(f32[32,256]{1,0:T(8,128)} %param.20) | copy-start | bytes 98308
  100.4 97.8 %copy-start.3 = (bf16[256,256]{1,0:T(8,128)(2,1)S(1)}, bf16[256,256]{1,0:T(8,128)(2,1)}, u32[]{:S(2)}) copy-start(bf16[256,256]{1,0:T(8,128)(2,1)} %param.16) | copy-start | bytes 393220
  100.4 181.0 %all-gather.11.cloned.1.call-start = ((), (), s32[]{:S(2)}) async-start(), calls=%async_computation.5 | async-start | bytes 1179648 | tf_op jit(solution)/shard_map/all_gather | solution.py:58
  166.1 33.2 %copy-start.4 = (bf16[256,256]{1,0:T(8,128)(2,1)S(1)}, bf16[256,256]{1,0:T(8,128)(2,1)}, u32[]{:S(2)}) copy-start(bf16[256,256]{1,0:T(8,128)(2,1)} %param.17) | copy-start | bytes 393220
  240.8 116.8 %all-gather.9.cloned.1.call-start = ((), (), s32[]{:S(2)}) async-start(), calls=%async_computation.4 | async-start | bytes 4718592 | tf_op jit(solution)/shard_map/all_gather | solution.py:57
  246.6 7.8 %copy-start.1 = (f32[256,1024]{0,1:T(8,128)S(1)}, f32[256,1024]{0,1:T(8,128)}, u32[]{:S(2)}) copy-start(f32[256,1024]{0,1:T(8,128)} %get-tuple-element.21) | copy-start | bytes 3145732
Sparse Core Ops, SparseCore 0:
  10.1 42.9 all-gather.4
  55.3 38.9 all-gather.6
  100.5 63.7 reduce-scatter.1
  240.9 40.4 all-gather.10
  283.9 73.6 all-gather.8
where the time goes:
time: 371 us; the launch traced here: 370 us
  waiting for transfers between devices  243 us (65%)
  blocking collectives  69.6 us (19%)
  local copies, waits for them, and re-layouts  22 us (6%)
  between operations  15.3 us (4%)
  matrix products  13.3 us (4%)
  other arithmetic  7.18 us (2%)
    all_gather x1, waiting for transfers between devices, per_device(): lax.all_gather(gate_new.astype(jnp.bfloat16), 'fs', axis=0, tiled=True)  73.9 us
    reduce_scatter x1, waiting for transfers between devices, per_device(): lax.psum_scatter(partial_proj, 'fs', scatter_dimension=0, tiled=True)  62.2 us
    all_gather x1, waiting for transfers between devices, per_device(): lax.all_gather(gate_factor, 'fs', axis=0, tiled=True)  44.4 us
    psum x1, blocking collectives, per_device(): lax.psum((jnp.sum(gate_full * gate_full), jnp.sum(state_full * state_full...  37.5 us
    all_gather x1, waiting for transfers between devices, per_device(): lax.all_gather(state_factor, 'fs', axis=0, tiled=True)  35.3 us
    all_gather x1, blocking collectives, per_device(): all_dirs = lax.all_gather(direction, 'fs', axis=0, tiled=True)  32.1 us
    all_gather x1, waiting for transfers between devices, per_device(): lax.all_gather(state_new.astype(jnp.bfloat16), 'fs', axis=0, tiled=True)  25.7 us
    unnamed x26, local copies, waits for them, and re-layouts  16 us
  transfers between devices with their start and end apart: 5, of which 5 were waited for; matrix products, arithmetic and copies ran while one was open for 6% of the time, Pallas kernels for 0%

commit v1 on v0

--- a/solution.py
+++ b/solution.py
@@ -2,6 +2,7 @@
 import jax.numpy as jnp
 from jax import lax
 from jax.sharding import PartitionSpec as P
+from jax.lax import psum
 
 D = 2048
 DI = 4096
@@ -46,8 +47,8 @@
     all_dirs = lax.all_gather(direction, "fs", axis=0, tiled=True)
     gate_full = jnp.dot(gate_factor, all_dirs[:, :gate_cols], preferred_element_type=jnp.float32)
     state_full = jnp.dot(state_factor, all_dirs[:, gate_cols:], preferred_element_type=jnp.float32)
-    gate_sq, state_sq = lax.psum(
-        (jnp.sum(gate_full * gate_full), jnp.sum(state_full * state_full)), ("fs", "tp")
+    gate_sq, state_sq = psum(
+        psum((jnp.sum(gate_full * gate_full), jnp.sum(state_full * state_full)), "tp"), "fs"
     )
     gate_scale = 0.02 / jnp.sqrt(gate_sq / (D * DI) + 0.25)
     state_scale = 0.02 / jnp.sqrt(state_sq / (D * BW) + 0.25)

time: 371 us -> 356 us (0.960)
  blocking collectives: 69.6 us -> 57.9 us
  waiting for transfers between devices: 243 us -> 239 us
    psum x1 -> x2, blocking collectives: 37.5 us -> 25.8 us  [the longest x1 19.6 us: per_device(): psum(psum((jnp.sum(gate_full * gate_full), jnp.sum(state_full * state_ful...]
where the time goes in v1:
time: 356 us; the launch traced here: 355 us
  waiting for transfers between devices  239 us (67%)
  blocking collectives  57.9 us (16%)
  local copies, waits for them, and re-layouts  22 us (6%)
  between operations  15.3 us (4%)
  matrix products  13.3 us (4%)
  other arithmetic  7.2 us (2%)
    all_gather x1, waiting for transfers between devices, per_device(): lax.all_gather(gate_new.astype(jnp.bfloat16), 'fs', axis=0, tiled=True)  73.9 us
    reduce_scatter x1, waiting for transfers between devices, per_device(): lax.psum_scatter(partial_proj, 'fs', scatter_dimension=0, tiled=True)  62.2 us
    all_gather x1, waiting for transfers between devices, per_device(): lax.all_gather(gate_factor, 'fs', axis=0, tiled=True)  44.4 us
    all_gather x1, waiting for transfers between devices, per_device(): lax.all_gather(state_factor, 'fs', axis=0, tiled=True)  35.3 us
    all_gather x1, blocking collectives, per_device(): all_dirs = lax.all_gather(direction, 'fs', axis=0, tiled=True)  32.1 us
    all_gather x1, waiting for transfers between devices, per_device(): lax.all_gather(state_new.astype(jnp.bfloat16), 'fs', axis=0, tiled=True)  22.2 us
    psum x1, blocking collectives, per_device(): psum(psum((jnp.sum(gate_full * gate_full), jnp.sum(state_full * state_ful...  19.6 us
    unnamed x26, local copies, waits for them, and re-layouts  16 us
  transfers between devices with their start and end apart: 5, of which 5 were waited for; matrix products, arithmetic and copies ran while one was open for 6% of the time, Pallas kernels for 0%

profile of v1, /device:TPU:0, one launch (start us, length us, event | category | flops | bytes accessed | tf_op | source)
XLA Modules:
  0.0 355.3 jit_solution(6174143175390339941)
XLA Ops:
  7.2 0.7 all-gather.5.cloned.1.call-update
  8.0 0.7 all-gather.7.cloned.1.call-update
  8.7 44.4 %all-gather.5.cloned.1.call-done = bf16[2048,256]{1,0:T(8,128)(2,1)} async-done(((bf16[256,256]{1,0:T(8,128)(2,1)}), bf16[2048,256]{1,0:T(8,128)(2,1)}) %all-gather.5.cloned.1.call-update) | async-done | bytes 1048592 | tf_op jit(solution)/shard_map/all_gather | solution.py:35
  53.2 4.1 %fusion.16 = f32[1152,256]{1,0:T(8,128)S(1)} fusion(bf16[1152,2048]{1,0:T(8,128)(2,1)} %param.11, bf16[2048,256]{1,0:T(8,128)(2,1)} %all-gather.5.cloned.1.call-done), kind=kOutput, calls=%fused_computation.27 | convolution fusion | flops 1207959552 | bytes 6946816 | tf_op jit(solution)/shard_map/dot_general | solution.py:13
  57.2 0.9 fusion.6
  58.1 0.9 convolution_add_fusion
  59.0 35.3 %all-gather.7.cloned.1.call-done = bf16[2048,256]{1,0:T(8,128)(2,1)} async-done(((bf16[256,256]{1,0:T(8,128)(2,1)}), bf16[2048,256]{1,0:T(8,128)(2,1)}) %all-gather.7.cloned.1.call-update) | async-done | bytes 1048592 | tf_op jit(solution)/shard_map/all_gather | solution.py:36
  94.3 4.1 %fusion.17 = f32[1152,256]{1,0:T(8,128)S(1)} fusion(bf16[1152,2048]{1,0:T(8,128)(2,1)} %param.11, bf16[2048,256]{1,0:T(8,128)(2,1)} %all-gather.7.cloned.1.call-done), kind=kOutput, calls=%fused_computation.28 | convolution fusion | flops 1207959552 | bytes 6946816 | tf_op jit(solution)/shard_map/dot_general | solution.py:13
  98.4 0.4 fusion.3
  99.2 1.2 pad_maximum_fusion
  100.4 0.8 copy-done.5
  101.3 0.8 copy.22
  102.1 62.2 %reduce-scatter.2.cloned.1.call-done = f32[32,1280]{1,0:T(8,128)} async-done(((f32[256,1280]{1,0:T(8,128)}), f32[32,1280]{1,0:T(8,128)}) %reduce-scatter.2.cloned.1.call-update) | async-done | bytes 163856 | tf_op jit(solution)/shard_map/reduce_scatter | solution.py:41
  164.4 1.7 multiply_convert_fusion
  166.1 32.1 %all_gather.17 = bf16[256,1280]{1,0:T(8,128)(2,1)S(1)} all-gather(bf16[32,1280]{1,0:T(8,128)(2,1)S(1)} %get-tuple-element.24), channel_id=1, replica_groups=mesh['fs'=8,'tp'=4] {'fs'}, dimensions={0}, use_global_device_ids=true | all-gather | bytes 737280 | tf_op jit(solution)/shard_map/all_gather | solution.py:47
  198.2 1.1 multiply_reduce_fusion
  199.2 1.5 multiply_reduce_fusion.1
  200.8 6.3 %all-reduce.1 = (f32[]{:T(128)}, f32[]{:T(128)}) all-reduce(f32[]{:T(128)} %get-tuple-element.27, f32[]{:T(128)} %get-tuple-element.29), channel_id=1, replica_groups=mesh['fs'=8,'tp'=4] {'tp'}, use_global_device_ids=true, to_apply=%region_2.0 | all-reduce | flops 2 | bytes 16 | tf_op jit(solution)/shard_map/psum | solution.py:51
  207.0 19.6 %all-reduce = (f32[]{:T(128)}, f32[]{:T(128)}) all-reduce(f32[]{:T(128)} %get-tuple-element.18, f32[]{:T(128)} %get-tuple-element.19), channel_id=1, replica_groups=mesh['fs'=8,'tp'=4] {'fs'}, use_global_device_ids=true, to_apply=%region_3.0 | all-reduce | flops 2 | bytes 16 | tf_op jit(solution)/shard_map/psum | solution.py:50
  227.3 1.8 fusion.12
  229.2 2.5 copy.21
  232.4 2.5 fusion.13
  235.0 1.7 slice.26
  236.6 1.4 slice.28
  238.0 1.6 slice.27
  239.6 1.4 slice.29
  240.9 1.8 copy.24
  242.7 1.3 copy.23
  244.0 22.2 %all-gather.11.cloned.1.call-done = bf16[2048,256]{0,1:T(8,128)(2,1)} async-done(((bf16[256,256]{0,1:T(8,128)(2,1)}), bf16[2048,256]{0,1:T(8,128)(2,1)}) %all-gather.11.cloned.1.call-update) | async-done | bytes 1048592 | tf_op jit(solution)/shard_map/all_gather | solution.py:59
  266.2 2.3 copy.26
  268.4 73.9 %all-gather.9.cloned.1.call-done = bf16[2048,1024]{0,1:T(8,128)(2,1)} async-done(((bf16[256,1024]{0,1:T(8,128)(2,1)}), bf16[2048,1024]{0,1:T(8,128)(2,1)}) %all-gather.9.cloned.1.call-update) | async-done | bytes 4194320 | tf_op jit(solution)/shard_map/all_gather | solution.py:58
  342.3 6.4 %copy.25 = bf16[2048,1024]{1,0:T(8,128)(2,1)} copy(bf16[2048,1024]{0,1:T(8,128)(2,1)} %all-gather.9.cloned.1.call-done) | data formatting | bytes 8388608
  (28 shorter events, 0.7 us)
Async XLA Ops:
  7.2 50.0 %copy-start = (bf16[1152,1024]{1,0:T(8,128)(2,1)S(1)}, bf16[1152,1024]{1,0:T(8,128)(2,1)}, u32[]{:S(2)}) copy-start(bf16[1152,1024]{1,0:T(8,128)(2,1)} %param.12) | copy-start | bytes 7077892
  7.2 46.0 %all-gather.5.cloned.1.call-start = ((), (), s32[]{:S(2)}) async-start(), calls=%async_computation.1 | async-start | bytes 1179648 | tf_op jit(solution)/shard_map/all_gather | solution.py:35
  7.9 86.4 %all-gather.7.cloned.1.call-start = ((), (), s32[]{:S(2)}) async-start(), calls=%async_computation.2 | async-start | bytes 1179648 | tf_op jit(solution)/shard_map/all_gather | solution.py:36
  8.7 155.7 %reduce-scatter.2.cloned.1.call-start = ((), (), s32[]{:S(2)}) async-start(), calls=%async_computation.3 | async-start | bytes 1474560 | tf_op jit(solution)/shard_map/reduce_scatter | solution.py:41
  94.3 4.1 %copy-start.2 = (bf16[1152,256]{1,0:T(8,128)(2,1)S(1)}, bf16[1152,256]{1,0:T(8,128)(2,1)}, u32[]{:S(2)}) copy-start(bf16[1152,256]{1,0:T(8,128)(2,1)} %param.13) | copy-start | bytes 1769476
  100.3 0.9 copy-start.5
  100.3 64.0 %copy-start.6 = (f32[32,1024]{1,0:T(8,128)S(1)}, f32[32,1024]{1,0:T(8,128)}, u32[]{:S(2)}) copy-start(f32[32,1024]{1,0:T(8,128)} %param.19) | copy-start | bytes 393220
  100.3 64.0 %copy-start.7 = (f32[32,1024]{1,0:T(8,128)S(1)}, f32[32,1024]{1,0:T(8,128)}, u32[]{:S(2)}) copy-start(f32[32,1024]{1,0:T(8,128)} %param.18) | copy-start | bytes 393220
  100.3 64.0 %copy-start.8 = (f32[32,256]{1,0:T(8,128)S(1)}, f32[32,256]{1,0:T(8,128)}, u32[]{:S(2)}) copy-start(f32[32,256]{1,0:T(8,128)} %param.21) | copy-start | bytes 98308
  100.3 64.0 %copy-start.9 = (f32[32,256]{1,0:T(8,128)S(1)}, f32[32,256]{1,0:T(8,128)}, u32[]{:S(2)}) copy-start(f32[32,256]{1,0:T(8,128)} %param.20) | copy-start | bytes 98308
  100.4 97.8 %copy-start.3 = (bf16[256,256]{1,0:T(8,128)(2,1)S(1)}, bf16[256,256]{1,0:T(8,128)(2,1)}, u32[]{:S(2)}) copy-start(bf16[256,256]{1,0:T(8,128)(2,1)} %param.16) | copy-start | bytes 393220
  100.4 165.8 %all-gather.11.cloned.1.call-start = ((), (), s32[]{:S(2)}) async-start(), calls=%async_computation.5 | async-start | bytes 1179648 | tf_op jit(solution)/shard_map/all_gather | solution.py:59
  166.1 33.2 %copy-start.4 = (bf16[256,256]{1,0:T(8,128)(2,1)S(1)}, bf16[256,256]{1,0:T(8,128)(2,1)}, u32[]{:S(2)}) copy-start(bf16[256,256]{1,0:T(8,128)(2,1)} %param.17) | copy-start | bytes 393220
  229.1 113.2 %all-gather.9.cloned.1.call-start = ((), (), s32[]{:S(2)}) async-start(), calls=%async_computation.4 | async-start | bytes 4718592 | tf_op jit(solution)/shard_map/all_gather | solution.py:58
  234.9 7.8 %copy-start.1 = (f32[256,1024]{0,1:T(8,128)S(1)}, f32[256,1024]{0,1:T(8,128)}, u32[]{:S(2)}) copy-start(f32[256,1024]{0,1:T(8,128)} %get-tuple-element.23) | copy-start | bytes 3145732
Sparse Core Ops, SparseCore 0:
  10.1 42.9 all-gather.4
  55.3 38.9 all-gather.6
  100.5 63.7 reduce-scatter.1
  229.3 36.8 all-gather.10
  268.7 73.6 all-gather.8
